TPU v7x, 32 devices: a whole 2x2x4 slice. The times are simulated.
32 devices in a mesh: sp: 16 (over z, x, core), tp: 2 (over y).
Axes of the slice: x: 2, y: 2, z: 4, core: 2. Of those that a mesh axis runs over, the one named last changes fastest.
Arguments:
- residual: bfloat16 [4096, 2048], P(('sp', 'tp')), may hold values from -6 to 6
- query_vectors: bfloat16 [4096, 512], P('sp', 'tp'), may hold values from -6 to 6
- key_vectors: bfloat16 [4096, 512], P('sp', 'tp'), may hold values from -6 to 6
- value_vectors: bfloat16 [4096, 512], P('sp', 'tp'), may hold values from -6 to 6
- in_gate: float32 [8, 4096], P('tp', 'sp'), may hold values from -9 to 190
- forget_gate: float32 [8, 4096], P('tp', 'sp'), may hold values from -1 to 12
- documents: int32 [4096], P('sp'), may hold values from 0 to 3, never falling along the last dimension, each value on 1 to 2048 neighbouring positions
- w_out: bfloat16 [512, 2048], P('tp'), may hold values from -0.25 to 0.25
- norm_gain: bfloat16 [2048], replicated, may hold values from 0.099609375 to 1.8984375
- w_up: bfloat16 [2048, 8192], P('sp', 'tp'), may hold values from -0.125 to 0.125
- w_down: bfloat16 [8192, 2048], P('tp', 'sp'), may hold values from -0.0625 to 0.0625
Outputs:
- layer_out: bfloat16 [4096, 2048], P(('sp', 'tp'))
Inputs may be any that keep to these rules, and one draw needn't show every extreme that they name: `documents`: document numbers never fall along the positions; every document has 1 to 2048 positions.
All inputs are finite; a program needn't handle non-finite values.
Results may differ from a plain program's by a relative error of at most 0.015.
Values may be sent and summed in bfloat16 or wider, within the bound.
A program may use at most 128 MiB of HBM per device.

v0:
```python
import jax
import jax.numpy as jnp
import numpy as np
from jax import lax
from jax.sharding import Mesh, PartitionSpec as P

DOC_MOST = 2048
very_negative = -1e30
epsilon = 1e-06
SP = ("z", "g")


def combine(earlier, later):
    memory_one, top_one, decay_one, first_one, last_one = earlier
    memory_two, top_two, decay_two, first_two, last_two = later
    later_empty = first_two < 0.0
    earlier_empty = first_one < 0.0
    keep = later_empty | (first_two == last_two) & (first_two == last_one)
    decay_step = jnp.where(later_empty, 0.0, decay_two)
    top_new = jnp.where(keep, jnp.maximum(decay_step + top_one, top_two), top_two)
    scale_old = jnp.where(keep, jnp.exp(decay_step + top_one - top_new), 0.0)
    scale_new = jnp.exp(top_two - top_new)
    memory_new = scale_old[:, None, None] * memory_one + scale_new[:, None, None] * memory_two
    decay_new = jnp.where(keep, decay_one + decay_step, decay_two)
    first_new = jnp.where(earlier_empty, first_two, first_one)
    last_new = jnp.where(later_empty, last_one, last_two)
    return (memory_new, top_new, decay_new, first_new, last_new)


def pack(state):
    memory, top, decay, first, last = state
    heads, _, width = memory.shape
    row = jnp.stack(
        [top, decay, jnp.broadcast_to(first, top.shape), jnp.broadcast_to(last, top.shape)], axis=1
    )
    row = jnp.pad(row, ((0, 0), (0, width - 4)))
    return jnp.concatenate(
        [memory, row[:, None, :], jnp.zeros((heads, 6, width), jnp.float32)], axis=1
    )


def unpack(packed, present):
    rows = packed.shape[1] - 7
    row = packed[:, rows]
    memory = jnp.where(present, packed[:, :rows], 0.0)
    top = jnp.where(present, row[:, 0], very_negative)
    decay = jnp.where(present, row[:, 1], 0.0)
    first = jnp.where(present, row[0, 2], -1.0)
    last = jnp.where(present, row[0, 3], -1.0)
    return (memory, top, decay, first, last)


def shifted(state, distance, length, here):
    packed = lax.ppermute(pack(state), SP, [(i, i + distance) for i in range(length - distance)])
    return unpack(packed, here >= distance)


def on_device(
    residual,
    query_vectors,
    key_vectors,
    value_vectors,
    in_gate,
    forget_gate,
    documents,
    w_out,
    norm_gain,
    w_up,
    w_down,
):
    tok_rows = query_vectors.shape[0]
    heads = in_gate.shape[0]
    head_dim = query_vectors.shape[1] // heads
    length = lax.axis_size(SP)
    here = lax.axis_index(SP)
    tp = lax.axis_size("tp")
    me = lax.axis_index("tp")
    up_part = lax.all_to_all(w_up, "g", split_axis=1, concat_axis=0, tiled=True)
    down_part = lax.all_to_all(w_down, "g", split_axis=0, concat_axis=1, tiled=True)
    up_all = lax.all_gather(up_part, "z", axis=0, tiled=True)

    def turn(value, d):
        return lax.ppermute(value, "tp", [(i, (i + d) % tp) for i in range(tp)])

    w_out_parts = [w_out] + [turn(w_out, d) for d in range(1, tp)]
    segment = documents.astype(jnp.float32)
    decay_log = jax.nn.log_sigmoid(forget_gate)
    cumulative = jnp.cumsum(decay_log, axis=-1)
    key_heads = jnp.transpose(key_vectors.reshape(tok_rows, heads, head_dim), (1, 0, 2))
    value_heads = jnp.transpose(value_vectors.reshape(tok_rows, heads, head_dim), (1, 0, 2))
    query_heads = jnp.transpose(query_vectors.reshape(tok_rows, heads, head_dim), (1, 0, 2))
    query_heads = query_heads * jnp.asarray(head_dim ** (-0.5), query_heads.dtype)
    latest = segment == segment[-1]
    growth = jnp.where(latest[None, :], cumulative[:, -1:] - cumulative + in_gate, very_negative)
    top_log = jnp.max(growth, axis=-1)
    summary_weight = jnp.exp(growth - top_log[:, None])
    key_wide = key_heads.astype(jnp.float32)
    weighted = key_wide * summary_weight[:, :, None]
    memory = jnp.einsum(
        "hsv,hsk->hvk", value_heads.astype(jnp.float32), weighted, precision=lax.Precision.HIGHEST
    )
    normal = jnp.sum(weighted, axis=1)
    state = (
        jnp.concatenate([memory, normal[:, None, :]], axis=1),
        top_log,
        cumulative[:, -1],
        segment[0],
        segment[-1],
    )
    reach = min(length - 1, -(-(DOC_MOST - 1) // tok_rows))
    span = 1
    while span < reach:
        state = combine(shifted(state, span, length, here), state)
        span *= 2
    incoming = shifted(state, 1, length, here)
    memory_in, top_in, _, _, last_in = incoming
    row_ids = lax.broadcasted_iota(jnp.int32, (tok_rows, tok_rows), 0)
    col_ids = lax.broadcasted_iota(jnp.int32, (tok_rows, tok_rows), 1)
    allowed = (col_ids <= row_ids) & (segment[:, None] == segment[None, :])
    inside = jnp.where(
        allowed[None],
        cumulative[:, :, None] - cumulative[:, None, :] + in_gate[:, None, :],
        very_negative,
    )
    peak_inside = jnp.max(inside, axis=-1)
    scores = jnp.einsum("hld,hsd->hls", query_heads, key_heads, preferred_element_type=jnp.float32)
    weight_inside = jnp.exp(inside - peak_inside[:, :, None]) * scores
    from_block = jnp.einsum(
        "hls,hsv->hlv",
        weight_inside.astype(jnp.bfloat16),
        value_heads,
        preferred_element_type=jnp.float32,
    )
    sum_inside = jnp.sum(weight_inside, axis=-1)
    outside = jnp.where((segment == last_in)[None, :], cumulative + top_in[:, None], very_negative)
    peak_log = jnp.maximum(outside, peak_inside)
    carried = jnp.exp(outside - peak_log)
    local = jnp.exp(peak_inside - peak_log)
    readout = jnp.einsum(
        "hlk,hvk->hlv", query_heads.astype(jnp.float32), memory_in, precision=lax.Precision.HIGHEST
    )
    numer = carried[:, :, None] * readout[:, :, :head_dim] + local[:, :, None] * from_block
    denom = carried * readout[:, :, head_dim] + local * sum_inside
    mixed = numer / jnp.maximum(jnp.abs(denom), jnp.exp(-peak_log))[:, :, None]
    mixed = jnp.transpose(mixed, (1, 0, 2)).reshape(tok_rows, -1).astype(jnp.bfloat16)
    own_rows = tok_rows // tp
    mixed_rows = mixed.reshape(tp, own_rows, -1)
    projected = 0.0
    for d in range(tp):
        piece = lax.dynamic_index_in_dim(mixed_rows, (me + d) % tp, 0, keepdims=False)
        if d:
            piece = turn(piece, d)
        projected = projected + jnp.dot(piece, w_out_parts[d], preferred_element_type=jnp.float32)
    middle = (residual.astype(jnp.float32) + projected).astype(jnp.bfloat16)
    middle_wide = middle.astype(jnp.float32)
    factor = lax.rsqrt(jnp.mean(middle_wide * middle_wide, axis=-1, keepdims=True) + epsilon)
    normed = (middle_wide * factor * norm_gain.astype(jnp.float32)).astype(jnp.bfloat16)
    gathered = lax.all_gather(normed, ("g", "tp"), axis=0, tiled=True)
    down_all = lax.all_gather(down_part, "z", axis=1, tiled=True)
    lifted = jnp.dot(gathered, up_all, preferred_element_type=jnp.float32)
    hidden = jnp.square(jax.nn.relu(lifted)).astype(jnp.bfloat16)
    terms = jnp.dot(hidden, down_all, preferred_element_type=jnp.float32)
    summed = lax.psum_scatter(
        terms.astype(jnp.bfloat16), ("g", "tp"), scatter_dimension=0, tiled=True
    ).astype(jnp.float32)
    return (middle_wide + summed).astype(jnp.bfloat16)


def solution(mesh):
    sp, tp = (mesh.shape["sp"], mesh.shape["tp"])
    plane = min(sp, 2 * tp)
    if sp % plane:
        plane = 1
    split = Mesh(np.asarray(mesh.devices).reshape(sp // plane, plane, tp), ("z", "g", "tp"))
    placed = (
        P(("z", "g", "tp"), None),
        P(SP, "tp"),
        P(SP, "tp"),
        P(SP, "tp"),
        P("tp", SP),
        P("tp", SP),
        P(SP),
        P("tp", None),
        P(),
        P(SP, "tp"),
        P("tp", SP),
    )
    return jax.shard_map(
        on_device, mesh=split, in_specs=placed, out_specs=P(("z", "g", "tp"), None), check_vma=False
    )
```

profile of v0, /device:TPU:0, one launch (start us, length us, event | category | flops | bytes accessed | tf_op | source)
XLA Modules:
  0.0 308.7 jit_solution(7243872329865839913)
XLA Ops:
  6.6 18.8 %all_to_all.38 = bf16[4,1024,128]{2,1,0:T(8,128)(2,1)S(1)} all-to-all(bf16[4,1024,128]{2,1,0:T(8,128)(2,1)} %bitcast.89), channel_id=1, replica_groups=mesh['z'=4,'g'=4,'tp'=2] {'g'}, dimensions={0} | all-to-all | bytes 2097152 | tf_op jit(solution)/shard_map/all_to_all | solution.py:79
  25.4 1.4 copy.209
  26.9 0.6 fusion.47
  27.5 0.6 pad.46.clone
  28.1 0.7 pad.47.clone
  28.9 1.2 reduce-window.6
  30.2 0.1 copy.191
  30.5 0.6 broadcast_compare_fusion.1
  31.1 0.2 slice_reduce_fusion.4
  31.3 0.2 fusion.42
  31.7 0.1 copy.196
  32.0 0.1 fusion.7
  32.1 0.1 copy.195
  32.2 1.0 copy.193
  33.3 0.3 convolution_bitcast_fusion
  33.5 0.1 maximum_maximum_fusion
  33.7 2.0 collective-permute-start
  35.7 1.3 copy.207
  37.0 4.7 %all-to-all-start = ((bf16[128,4,1024]{0,2,1:T(8,128)(2,1)}), bf16[128,4,1024]{0,2,1:T(8,128)(2,1)S(1)}, u32[]{:S(2)}, u32[]{:S(2)}) async-start(bf16[128,4,1024]{0,2,1:T(8,128)(2,1)} %bitcast.30), calls=%async_computation | async-start | bytes 2097152 | tf_op jit(solution)/shard_map/all_to_all | solution.py:78
  41.7 1.6 collective-permute-start.5
  43.4 0.1 fusion.9
  45.3 1.1 slice_reduce_fusion.3
  46.3 0.7 fusion.46
  50.2 0.2 fusion.33
  50.5 0.1 copy.200
  50.7 1.0 fusion.16
  51.7 0.1 maximum_maximum_fusion.1
  51.8 3.9 %collective-permute-start.1 = (f32[4,72,64]{1,2,0:T(8,128)S(1)}, f32[4,72,64]{1,2,0:T(8,128)S(1)}, u32[]{:S(2)}, u32[]{:S(2)}) collective-permute-start(f32[4,72,64]{1,2,0:T(8,128)S(1)} %maximum_maximum_fusion.1), channel_id=1, source_target_pairs={{0,4},{2,6},{4,8},{6,10},{8,12},{10,14},{12,16},{14,18},{16,20},{1... | collective-permute-start | bytes 221192 | tf_op jit(solution)/shard_map/ppermute | solution.py:54
  55.7 0.4 fusion.3
  56.1 3.0 collective-permute-done.1
  59.0 0.2 slice_reduce_fusion.2
  59.2 0.7 fusion.45
  60.5 1.3 copy.208
  61.9 0.2 fusion.35
  63.0 0.1 copy.201
  63.3 8.0 %collective-permute-start.2 = (f32[4,72,64]{1,2,0:T(8,128)S(1)}, f32[4,72,64]{1,2,0:T(8,128)S(1)}, u32[]{:S(2)}, u32[]{:S(2)}) collective-permute-start(f32[4,72,64]{1,2,0:T(8,128)S(1)} %maximum_maximum_fusion.2), channel_id=1, source_target_pairs={{0,8},{2,10},{4,12},{6,14},{8,16},{10,18},{12,20},{14,22},{16,24},... | collective-permute-start | bytes 221192 | tf_op jit(solution)/shard_map/ppermute | solution.py:54
  71.3 0.5 fusion.48
  71.9 5.7 %collective-permute-done.2 = f32[4,72,64]{1,2,0:T(8,128)S(1)} collective-permute-done((f32[4,72,64]{1,2,0:T(8,128)S(1)}, f32[4,72,64]{1,2,0:T(8,128)S(1)}, u32[]{:S(2)}, u32[]{:S(2)}) %collective-permute-start.2) | collective-permute-done | bytes 73760 | tf_op jit(solution)/shard_map/ppermute | solution.py:54
  77.6 0.2 slice_reduce_fusion.1
  77.7 0.7 fusion.44
  79.9 0.1 maximum_select_fusion
  80.1 0.1 copy.202
  80.4 0.1 maximum_maximum_fusion.3
  80.5 1.3 collective-permute-start.3
  81.9 0.9 collective-permute-done.3
  82.7 0.2 slice_reduce_fusion
  82.9 0.6 slice.113
  84.2 0.1 select_reduce_fusion
  84.3 0.3 fusion.10
  84.9 0.2 fusion.19
  85.1 0.3 constant_dynamic-slice_fusion
  85.4 0.1 copy.213
  85.5 0.1 copy.212
  85.6 0.6 collective-permute-start.4
  86.3 0.3 fusion.23
  86.6 3.4 %collective-permute-done.4 = bf16[128,256]{1,0:T(8,128)(2,1)S(1)} collective-permute-done((bf16[128,256]{1,0:T(8,128)(2,1)S(1)}, bf16[128,256]{1,0:T(8,128)(2,1)S(1)}, u32[]{:S(2)}, u32[]{:S(2)}) %collective-permute-start.4) | collective-permute-done | bytes 65568 | tf_op jit(solution)/shard_map/ppermute | solution.py:83
  90.0 1.6 multiply_reduce_fusion
  91.6 1.0 multiply_convert_fusion.1
  92.7 16.1 %all-gather.8.cloned.1.call-done = bf16[1024,2048]{0,1:T(8,128)(2,1)} async-done(((bf16[1024,512]{0,1:T(8,128)(2,1)}), bf16[1024,2048]{0,1:T(8,128)(2,1)}) %all-gather.8.cloned.1.call-update) | async-done | bytes 4194320 | tf_op jit(solution)/shard_map/all_gather | solution.py:159
  108.7 88.8 %all-gather.6.cloned.1.call-done = bf16[2048,1024]{1,0:T(8,128)(2,1)} async-done(((bf16[512,1024]{1,0:T(8,128)(2,1)}), bf16[2048,1024]{1,0:T(8,128)(2,1)}) %all-gather.6.cloned.1.call-update) | async-done | bytes 4194320 | tf_op jit(solution)/shard_map/all_gather | solution.py:80
  197.6 37.0 %all-gather.4.cloned.1.call-done = bf16[1024,2048]{1,0:T(8,128)(2,1)} async-done(((bf16[128,2048]{1,0:T(8,128)(2,1)}), bf16[1024,2048]{1,0:T(8,128)(2,1)}) %all-gather.4.cloned.1.call-update) | async-done | bytes 4194320 | tf_op jit(solution)/shard_map/all_gather | solution.py:158
  234.6 14.4 %convolution_convert_fusion = bf16[1024,2048]{1,0:T(8,128)(2,1)} fusion(bf16[1024,2048]{0,1:T(8,128)(2,1)} %all-gather.8.cloned.1.call-done, bf16[1024,2048]{1,0:T(8,128)(2,1)} %all-gather.4.cloned.1.call-done, bf16[2048,1024]{1,0:T(8,128)(2,1)} %all-gather.6.cloned.1.call-done), kind=kOutput, calls=%fused_computation.1 | convolution fusion | flops 8595177472 | bytes 16777216 | tf_op jit(solution)/shard_map/dot_general | solution.py:162
  249.0 51.3 %reduce-scatter.2.cloned.1.call-done = bf16[128,2048]{1,0:T(8,128)(2,1)} async-done(((bf16[1024,2048]{1,0:T(8,128)(2,1)}), bf16[128,2048]{1,0:T(8,128)(2,1)}) %reduce-scatter.2.cloned.1.call-update) | async-done | bytes 524304 | tf_op jit(solution)/shard_map/reduce_scatter | solution.py:163
  300.3 1.9 add_convert_fusion
  (80 shorter events, 2.5 us)
Async XLA Ops:
  6.5 20.3 %copy-start.8 = (s32[256]{0:T(256)S(1)}, s32[256]{0:T(256)}, u32[]{:S(2)}) copy-start(s32[256]{0:T(256)} %param.17) | copy-start | bytes 3076
  6.5 22.3 %copy-start.10 = (f32[4,256]{1,0:T(4,128)S(1)}, f32[4,256]{1,0:T(4,128)}, u32[]{:S(2)}) copy-start(f32[4,256]{1,0:T(4,128)} %param.16) | copy-start | bytes 12292
  6.5 24.8 %copy-start.7 = (f32[4,256]{1,0:T(4,128)S(1)}, f32[4,256]{1,0:T(4,128)}, u32[]{:S(2)}) copy-start(f32[4,256]{1,0:T(4,128)} %param.15) | copy-start | bytes 12292
  6.5 25.2 %copy-start.5 = (bf16[256,256]{1,0:T(8,128)(2,1)S(1)}, bf16[256,256]{1,0:T(8,128)(2,1)}, u32[]{:S(2)}) copy-start(bf16[256,256]{1,0:T(8,128)(2,1)} %param.13) | copy-start | bytes 393220
  6.5 29.2 %copy-start = (bf16[128,4096]{1,0:T(8,128)(2,1)S(1)}, bf16[128,4096]{1,0:T(8,128)(2,1)}, u32[]{:S(2)}) copy-start(bf16[128,4096]{1,0:T(8,128)(2,1)} %param.20) | copy-start | bytes 3145732
  6.5 102.2 %all-gather.8.cloned.1.call-start = ((), (), s32[]{:S(2)}) async-start(), calls=%async_computation.5 | async-start | bytes 5242880 | tf_op jit(solution)/shard_map/all_gather | solution.py:159
  25.4 16.3 %copy-start.1 = (bf16[256,2048]{1,0:T(8,128)(2,1)S(1)}, bf16[256,2048]{1,0:T(8,128)(2,1)}, u32[]{:S(2)}) copy-start(bf16[256,2048]{1,0:T(8,128)(2,1)} %param.18) | copy-start | bytes 3145732
  26.8 16.5 %copy-start.6 = (bf16[256,256]{1,0:T(8,128)(2,1)S(1)}, bf16[256,256]{1,0:T(8,128)(2,1)}, u32[]{:S(2)}) copy-start(bf16[256,256]{1,0:T(8,128)(2,1)} %param.12) | copy-start | bytes 393220
  33.2 3.7 %copy-start.2 = (bf16[256,256]{0,1:T(8,128)(2,1)}, bf16[256,256]{0,1:T(8,128)(2,1)S(1)}, u32[]{:S(2)}) copy-start(bf16[256,256]{0,1:T(8,128)(2,1)S(1)} %copy.193) | copy-start | bytes 393220
  33.7 11.6 %collective-permute-start = (f32[4,72,64]{1,2,0:T(8,128)S(1)}, f32[4,72,64]{1,2,0:T(8,128)}, u32[]{:S(2)}, u32[]{:S(2)}) collective-permute-start(f32[4,72,64]{1,2,0:T(8,128)S(1)} %maximum_maximum_fusion), channel_id=1, source_target_pairs={{0,2},{2,4},{4,6},{6,8},{8,10},{10,12},{12,14},{14,16},{16,18},{18... | collective-permute-start | bytes 221192 | tf_op jit(solution)/shard_map/ppermute | solution.py:54
  37.0 23.5 %all-to-all-start = ((bf16[128,4,1024]{0,2,1:T(8,128)(2,1)}), bf16[128,4,1024]{0,2,1:T(8,128)(2,1)S(1)}, u32[]{:S(2)}, u32[]{:S(2)}) async-start(bf16[128,4,1024]{0,2,1:T(8,128)(2,1)} %bitcast.30), calls=%async_computation | async-start | bytes 2097152 | tf_op jit(solution)/shard_map/all_to_all | solution.py:78
  41.7 155.9 %all-gather.6.cloned.1.call-start = ((), (), s32[]{:S(2)}) async-start(), calls=%async_computation.4 | async-start | bytes 5242880 | tf_op jit(solution)/shard_map/all_gather | solution.py:80
  41.7 48.3 %collective-permute-start.5 = (bf16[256,2048]{1,0:T(8,128)(2,1)S(1)}, bf16[256,2048]{1,0:T(8,128)(2,1)}, u32[]{:S(2)}, u32[]{:S(2)}) collective-permute-start(bf16[256,2048]{1,0:T(8,128)(2,1)S(1)} %copy-done.1), channel_id=1, source_target_pairs={{0,1},{1,0},{2,3},{3,2},{4,5},{5,4},{6,7},{7,6},{8,9},{9,8},{10,11... | collective-permute-start | bytes 3145736 | tf_op jit(solution)/shard_map/ppermute | solution.py:83
  51.7 30.2 %copy-start.9 = (bf16[2048]{0:T(1024)(128)(2,1)S(1)}, bf16[2048]{0:T(1024)(128)(2,1)}, u32[]{:S(2)}) copy-start(bf16[2048]{0:T(1024)(128)(2,1)} %param.19) | copy-start | bytes 12292
  51.8 7.2 %collective-permute-start.1 = (f32[4,72,64]{1,2,0:T(8,128)S(1)}, f32[4,72,64]{1,2,0:T(8,128)S(1)}, u32[]{:S(2)}, u32[]{:S(2)}) collective-permute-start(f32[4,72,64]{1,2,0:T(8,128)S(1)} %maximum_maximum_fusion.1), channel_id=1, source_target_pairs={{0,4},{2,6},{4,8},{6,10},{8,12},{10,14},{12,16},{14,18},{16,20},{1... | collective-permute-start | bytes 221192 | tf_op jit(solution)/shard_map/ppermute | solution.py:54
  60.5 24.4 %copy-start.3 = (bf16[256,256]{0,1:T(8,128)(2,1)S(1)}, bf16[256,256]{0,1:T(8,128)(2,1)}, u32[]{:S(2)}) copy-start(bf16[256,256]{0,1:T(8,128)(2,1)} %copy-done.2) | copy-start | bytes 393220
  61.8 172.7 %all-gather.4.cloned.1.call-start = ((), (), s32[]{:S(2)}) async-start(), calls=%async_computation.3 | async-start | bytes 4718592 | tf_op jit(solution)/shard_map/all_gather | solution.py:158
  63.3 14.2 %collective-permute-start.2 = (f32[4,72,64]{1,2,0:T(8,128)S(1)}, f32[4,72,64]{1,2,0:T(8,128)S(1)}, u32[]{:S(2)}, u32[]{:S(2)}) collective-permute-start(f32[4,72,64]{1,2,0:T(8,128)S(1)} %maximum_maximum_fusion.2), channel_id=1, source_target_pairs={{0,8},{2,10},{4,12},{6,14},{8,16},{10,18},{12,20},{14,22},{16,24},... | collective-permute-start | bytes 221192 | tf_op jit(solution)/shard_map/ppermute | solution.py:54
  71.3 18.7 %copy-start.4 = (bf16[128,2048]{1,0:T(8,128)(2,1)S(1)}, bf16[128,2048]{1,0:T(8,128)(2,1)}, u32[]{:S(2)}) copy-start(bf16[128,2048]{1,0:T(8,128)(2,1)} %param.11) | copy-start | bytes 1572868
  80.5 2.3 collective-permute-start.3
  85.6 4.3 %collective-permute-start.4 = (bf16[128,256]{1,0:T(8,128)(2,1)S(1)}, bf16[128,256]{1,0:T(8,128)(2,1)S(1)}, u32[]{:S(2)}, u32[]{:S(2)}) collective-permute-start(bf16[128,256]{1,0:T(8,128)(2,1)S(1)} %bitcast.94), channel_id=1, source_target_pairs={{0,1},{1,0},{2,3},{3,2},{4,5},{5,4},{6,7},{7,6},{8,9},{9,8},{10,11... | collective-permute-start | bytes 196616 | tf_op jit(solution)/shard_map/ppermute | solution.py:83
  92.6 207.6 %reduce-scatter.2.cloned.1.call-start = ((), (), s32[]{:S(2)}) async-start(), calls=%async_computation.6 | async-start | bytes 4718592 | tf_op jit(solution)/shard_map/reduce_scatter | solution.py:163
Sparse Core Ops, SparseCore 0:
  26.9 81.7 all-gather.7
  110.3 87.2 all-gather.5
  199.5 35.0 all-gather.3
  249.1 51.1 reduce-scatter.1
where the time goes:
time: 309 us
  waiting for transfers between devices  206 us (67%)
  starting transfers between devices  22.2 us (7%)
  between operations  21.6 us (7%)
  blocking collectives  18.8 us (6%)
  matrix products  17.7 us (6%)
  local copies, waits for them, and re-layouts  13.7 us (4%)
  other arithmetic  8.61 us (3%)
    all_gather x1, waiting for transfers between devices, on_device(): up_all = lax.all_gather(up_part, 'z', axis=0, tiled=True)  88.8 us
    reduce_scatter x1, waiting for transfers between devices, on_device(): lax.psum_scatter(terms.astype(jnp.bfloat16), ('g', 'tp'), scatter_dimensi...  51.3 us
    all_gather x1, waiting for transfers between devices, on_device(): gathered = lax.all_gather(normed, ('g', 'tp'), axis=0, tiled=True)  37 us
    all_to_all x1, blocking collectives, on_device(): lax.all_to_all(w_down, 'g', split_axis=0, concat_axis=1, tiled=True)  18.8 us
    all_gather x1, waiting for transfers between devices, on_device(): down_all = lax.all_gather(down_part, 'z', axis=1, tiled=True)  16.1 us
    ppermute x4, starting transfers between devices, shifted(): lax.ppermute(pack(state), SP, [(i, i + distance) for i in range(length -...  15.2 us
    dot_general x1, matrix products, on_device(): terms = jnp.dot(hidden, down_all, preferred_element_type=jnp.float32)  14.4 us
    ppermute x4, waiting for transfers between devices, shifted(): lax.ppermute(pack(state), SP, [(i, i + distance) for i in range(length -...  9.54 us
  transfers between devices with their start and end apart: 11, of which 8 were waited for; matrix products, arithmetic and copies ran while one was open for 7% of the time, Pallas kernels for 0%

commit v1 on v0

--- a/solution.py
+++ b/solution.py
@@ -76,7 +76,9 @@
     tp = lax.axis_size("tp")
     me = lax.axis_index("tp")
     up_part = lax.all_to_all(w_up, "g", split_axis=1, concat_axis=0, tiled=True)
-    down_part = lax.all_to_all(w_down, "g", split_axis=0, concat_axis=1, tiled=True)
+    down_part = jnp.concatenate(
+        lax.all_to_all(jnp.stack(jnp.split(w_down, lax.axis_size("g"), axis=0)), "g", 0, 0), axis=1
+    )
     up_all = lax.all_gather(up_part, "z", axis=0, tiled=True)
 
     def turn(value, d):

time: 309 us -> 310 us (level)
  waiting for transfers between devices: 206 us -> 199 us
  other arithmetic: 8.61 us -> 13.6 us
    all_gather x1, waiting for transfers between devices: 88.8 us -> 9.66 us  [on_device(): up_all = lax.all_gather(up_part, 'z', axis=0, tiled=True)]
    all_gather x1, waiting for transfers between devices: 16.1 us -> 88.8 us  [on_device(): down_all = lax.all_gather(down_part, 'z', axis=1, tiled=True)]
    unnamed x30 -> x56, local copies, waits for them, and re-layouts: 2.78 us -> 6.16 us
  transfers between devices with their start and end apart: 11 -> 11, of which waited for: 8 -> 8; matrix products, arithmetic and copies ran while one was open for 7% -> 9% of each run, Pallas kernels for 0% -> 0%
where the time goes in v1:
time: 310 us; the launch traced here: 309 us
  waiting for transfers between devices  199 us (64%)
  starting transfers between devices  21.6 us (7%)
  between operations  21.6 us (7%)
  matrix products  19.5 us (6%)
  blocking collectives  18.5 us (6%)
  local copies, waits for them, and re-layouts  15.6 us (5%)
  other arithmetic  13.6 us (4%)
    all_gather x1, waiting for transfers between devices, on_device(): down_all = lax.all_gather(down_part, 'z', axis=1, tiled=True)  88.8 us
    reduce_scatter x1, waiting for transfers between devices, on_device(): lax.psum_scatter(terms.astype(jnp.bfloat16), ('g', 'tp'), scatter_dimensi...  51.3 us
    all_gather x1, waiting for transfers between devices, on_device(): gathered = lax.all_gather(normed, ('g', 'tp'), axis=0, tiled=True)  37 us
    all_to_all x1, blocking collectives, on_device(): up_part = lax.all_to_all(w_up, 'g', split_axis=1, concat_axis=0, tiled=True)  18.5 us
    ppermute x4, starting transfers between devices, shifted(): lax.ppermute(pack(state), SP, [(i, i + distance) for i in range(length -...  15.4 us
    dot_general x1, matrix products, on_device(): terms = jnp.dot(hidden, down_all, preferred_element_type=jnp.float32)  14.4 us
    all_gather x1, waiting for transfers between devices, on_device(): up_all = lax.all_gather(up_part, 'z', axis=0, tiled=True)  9.66 us
    ppermute x4, waiting for transfers between devices, shifted(): lax.ppermute(pack(state), SP, [(i, i + distance) for i in range(length -...  8.69 us
  transfers between devices with their start and end apart: 11, of which 8 were waited for; matrix products, arithmetic and copies ran while one was open for 9% of the time, Pallas kernels for 0%

profile of v1, /device:TPU:0, one launch (start us, length us, event | category | flops | bytes accessed | tf_op | source)
XLA Modules:
  0.0 309.4 jit_solution(13836973348961497236)
XLA Ops:
  6.6 1.7 copy.229
  8.3 18.5 %all_to_all.24 = bf16[128,4,1024]{0,2,1:T(8,128)(2,1)S(1)} all-to-all(bf16[128,4,1024]{0,2,1:T(8,128)(2,1)S(1)} %bitcast.89), channel_id=1, replica_groups=mesh['z'=4,'g'=4,'tp'=2] {'g'}, dimensions={1} | all-to-all | bytes 2097152 | tf_op jit(solution)/shard_map/all_to_all | solution.py:78
  26.8 1.3 copy.230
  28.3 0.6 fusion.48
  28.9 0.7 pad.50.clone
  29.6 0.6 pad.51.clone
  30.2 1.2 reduce-window.6
  31.8 0.5 copy-done.9
  32.4 0.6 broadcast_compare_fusion.1
  33.0 0.2 slice_reduce_fusion.4
  33.2 0.2 fusion.42
  33.5 0.5 copy-done.11
  34.7 0.3 convolution_bitcast_fusion
  35.0 0.4 copy-done.3
  35.4 0.8 maximum_maximum_fusion
  36.2 2.2 collective-permute-start
  38.4 0.1 copy.239
  38.5 0.1 copy.241
  38.7 0.1 copy.240
  38.9 0.1 copy.242
  39.0 1.1 pad_maximum_fusion
  40.1 3.9 %all-to-all-start.1 = ((bf16[4,1024,128]{1,2,0:T(8,128)(2,1)}), bf16[4,1024,128]{1,2,0:T(8,128)(2,1)S(1)}, u32[]{:S(2)}, u32[]{:S(2)}) async-start(bf16[4,1024,128]{1,2,0:T(8,128)(2,1)} %pad_maximum_fusion), calls=%async_computation.1 | async-start | bytes 2097152 | tf_op jit(solution)/shard_map/all_to_all | solution.py:80
  44.1 1.6 collective-permute-start.5
  45.7 1.0 copy.225
  46.7 0.8 fusion.9
  49.4 1.1 slice_reduce_fusion.3
  50.4 0.6 fusion.47
  54.2 0.9 fusion.33
  55.2 0.1 copy.222
  55.3 0.7 broadcast_select_fusion.10
  56.0 0.6 subtract_exponential_fusion.3
  56.6 1.0 fusion.16
  57.6 0.7 maximum_maximum_fusion.1
  58.4 3.9 %collective-permute-start.1 = (f32[4,72,64]{1,2,0:T(8,128)S(1)}, f32[4,72,64]{1,2,0:T(8,128)S(1)}, u32[]{:S(2)}, u32[]{:S(2)}) collective-permute-start(f32[4,72,64]{1,2,0:T(8,128)S(1)} %maximum_maximum_fusion.1), channel_id=1, source_target_pairs={{0,4},{2,6},{4,8},{6,10},{8,12},{10,14},{12,16},{14,18},{16,20},{1... | collective-permute-start | bytes 221192 | tf_op jit(solution)/shard_map/ppermute | solution.py:54
  62.3 0.4 fusion.3
  62.7 2.9 collective-permute-done.1
  65.6 0.2 slice_reduce_fusion.2
  65.8 0.6 fusion.46
  67.0 1.0 copy-done
  68.0 0.2 fusion.35
  69.5 8.1 %collective-permute-start.2 = (f32[4,72,64]{1,2,0:T(8,128)S(1)}, f32[4,72,64]{1,2,0:T(8,128)S(1)}, u32[]{:S(2)}, u32[]{:S(2)}) collective-permute-start(f32[4,72,64]{1,2,0:T(8,128)S(1)} %maximum_maximum_fusion.2), channel_id=1, source_target_pairs={{0,8},{2,10},{4,12},{6,14},{8,16},{10,18},{12,20},{14,22},{16,24},... | collective-permute-start | bytes 221192 | tf_op jit(solution)/shard_map/ppermute | solution.py:54
  77.5 1.3 fusion.49
  78.9 4.9 %collective-permute-done.2 = f32[4,72,64]{1,2,0:T(8,128)S(1)} collective-permute-done((f32[4,72,64]{1,2,0:T(8,128)S(1)}, f32[4,72,64]{1,2,0:T(8,128)S(1)}, u32[]{:S(2)}, u32[]{:S(2)}) %collective-permute-start.2) | collective-permute-done | bytes 73760 | tf_op jit(solution)/shard_map/ppermute | solution.py:54
  83.8 0.2 slice_reduce_fusion.1
  84.0 0.6 fusion.45
  86.1 0.1 copy.224
  86.5 1.3 collective-permute-start.3
  87.9 0.9 collective-permute-done.3
  88.8 0.2 slice_reduce_fusion
  89.0 0.7 slice.113
  90.4 0.3 fusion.10
  90.9 1.3 fusion.19
  92.2 0.3 constant_dynamic-slice_fusion
  92.8 0.5 collective-permute-start.4
  93.3 0.3 fusion.23
  93.6 3.5 %collective-permute-done.4 = bf16[128,256]{1,0:T(8,128)(2,1)S(1)} collective-permute-done((bf16[128,256]{1,0:T(8,128)(2,1)S(1)}, bf16[128,256]{1,0:T(8,128)(2,1)S(1)}, u32[]{:S(2)}, u32[]{:S(2)}) %collective-permute-start.4) | collective-permute-done | bytes 65568 | tf_op jit(solution)/shard_map/ppermute | solution.py:85
  97.1 1.6 multiply_reduce_fusion
  98.8 1.0 multiply_convert_fusion.1
  99.8 9.7 %all-gather.6.cloned.1.call-done = bf16[2048,1024]{1,0:T(8,128)(2,1)} async-done(((bf16[512,1024]{1,0:T(8,128)(2,1)}), bf16[2048,1024]{1,0:T(8,128)(2,1)}) %all-gather.6.cloned.1.call-update) | async-done | bytes 4194320 | tf_op jit(solution)/shard_map/all_gather | solution.py:82
  109.4 88.8 %all-gather.8.cloned.1.call-done = bf16[1024,2048]{0,1:T(8,128)(2,1)} async-done(((bf16[1024,512]{0,1:T(8,128)(2,1)}), bf16[1024,2048]{0,1:T(8,128)(2,1)}) %all-gather.8.cloned.1.call-update) | async-done | bytes 4194320 | tf_op jit(solution)/shard_map/all_gather | solution.py:161
  198.3 37.0 %all-gather.4.cloned.1.call-done = bf16[1024,2048]{1,0:T(8,128)(2,1)} async-done(((bf16[128,2048]{1,0:T(8,128)(2,1)}), bf16[1024,2048]{1,0:T(8,128)(2,1)}) %all-gather.4.cloned.1.call-update) | async-done | bytes 4194320 | tf_op jit(solution)/shard_map/all_gather | solution.py:160
  235.3 14.4 %convolution_convert_fusion = bf16[1024,2048]{1,0:T(8,128)(2,1)} fusion(bf16[1024,2048]{0,1:T(8,128)(2,1)} %all-gather.8.cloned.1.call-done, bf16[1024,2048]{1,0:T(8,128)(2,1)} %all-gather.4.cloned.1.call-done, bf16[2048,1024]{1,0:T(8,128)(2,1)} %all-gather.6.cloned.1.call-done), kind=kOutput, calls=%fused_computation.1 | convolution fusion | flops 8595177472 | bytes 16777216 | tf_op jit(solution)/shard_map/dot_general | solution.py:164
  249.7 51.3 %reduce-scatter.2.cloned.1.call-done = bf16[128,2048]{1,0:T(8,128)(2,1)} async-done(((bf16[1024,2048]{1,0:T(8,128)(2,1)}), bf16[128,2048]{1,0:T(8,128)(2,1)}) %reduce-scatter.2.cloned.1.call-update) | async-done | bytes 524304 | tf_op jit(solution)/shard_map/reduce_scatter | solution.py:165
  301.0 1.9 add_convert_fusion
  (107 shorter events, 3.7 us)
Async XLA Ops:
  6.5 21.7 %copy-start.15 = (s32[256]{0:T(256)S(1)}, s32[256]{0:T(256)}, u32[]{:S(2)}) copy-start(s32[256]{0:T(256)} %param.17) | copy-start | bytes 3076
  6.5 23.7 %copy-start.21 = (f32[4,256]{1,0:T(4,128)S(1)}, f32[4,256]{1,0:T(4,128)}, u32[]{:S(2)}) copy-start(f32[4,256]{1,0:T(4,128)} %param.16) | copy-start | bytes 12292
  6.5 26.6 %copy-start.8 = (f32[4,256]{1,0:T(4,128)S(1)}, f32[4,256]{1,0:T(4,128)}, u32[]{:S(2)}) copy-start(f32[4,256]{1,0:T(4,128)} %param.15) | copy-start | bytes 12292
  6.5 27.6 %copy-start.6 = (bf16[256,256]{1,0:T(8,128)(2,1)S(1)}, bf16[256,256]{1,0:T(8,128)(2,1)}, u32[]{:S(2)}) copy-start(bf16[256,256]{1,0:T(8,128)(2,1)} %param.13) | copy-start | bytes 393220
  6.5 28.0 %copy-start.7 = (bf16[256,256]{1,0:T(8,128)(2,1)S(1)}, bf16[256,256]{1,0:T(8,128)(2,1)}, u32[]{:S(2)}) copy-start(bf16[256,256]{1,0:T(8,128)(2,1)} %param.14) | copy-start | bytes 393220
  6.5 31.8 %copy-start.1 = (bf16[4096,128]{1,0:T(8,128)(2,1)S(1)}, bf16[4096,128]{1,0:T(8,128)(2,1)}, u32[]{:S(2)}) copy-start(bf16[4096,128]{1,0:T(8,128)(2,1)} %param.21) | copy-start | bytes 3145732
  6.6 102.9 %all-gather.6.cloned.1.call-start = ((), (), s32[]{:S(2)}) async-start(), calls=%async_computation.4 | async-start | bytes 5242880 | tf_op jit(solution)/shard_map/all_gather | solution.py:82
  28.2 3.5 %copy-start.12 = (f32[256]{0:T(256)}, f32[256]{0:T(256)S(1)}, u32[]{:S(2)}) copy-start(f32[256]{0:T(256)S(1)} %convert_element_type.54) | copy-start | bytes 3076
  28.3 6.7 %copy-start.17 = (f32[72]{0:T(128)}, f32[72]{0:T(128)S(1)}, u32[]{:S(2)}) copy-start(f32[72]{0:T(128)S(1)} %pad.47.clone) | copy-start | bytes 868
  31.8 0.5 copy-start.9
  33.2 1.3 copy-start.13
  33.4 1.0 copy-start.19
  33.5 0.6 copy-start.11
  34.7 0.7 copy-start.3
  36.2 7.9 %copy-start.2 = (bf16[256,2048]{1,0:T(8,128)(2,1)S(1)}, bf16[256,2048]{1,0:T(8,128)(2,1)}, u32[]{:S(2)}) copy-start(bf16[256,2048]{1,0:T(8,128)(2,1)} %param.18) | copy-start | bytes 3145732
  36.2 13.2 %collective-permute-start = (f32[4,72,64]{1,2,0:T(8,128)}, f32[4,72,64]{1,2,0:T(8,128)}, u32[]{:S(2)}, u32[]{:S(2)}) collective-permute-start(f32[4,72,64]{1,2,0:T(8,128)} %maximum_maximum_fusion), channel_id=1, source_target_pairs={{0,2},{2,4},{4,6},{6,8},{8,10},{10,12},{12,14},{14,16},{16,18},{18... | collective-permute-start | bytes 221192 | tf_op jit(solution)/shard_map/ppermute | solution.py:54
  38.7 30.5 %copy-start.14 = (f32[4]{0:T(128)S(1)}, f32[4]{0:T(128)}, u32[]{:S(2)}) copy-start(f32[4]{0:T(128)} %copy-done.13) | copy-start | bytes 52
  38.9 30.5 %copy-start.18 = (f32[72]{0:T(128)S(1)}, f32[72]{0:T(128)}, u32[]{:S(2)}) copy-start(f32[72]{0:T(128)} %copy-done.17) | copy-start | bytes 868
  40.1 26.9 %all-to-all-start.1 = ((bf16[4,1024,128]{1,2,0:T(8,128)(2,1)}), bf16[4,1024,128]{1,2,0:T(8,128)(2,1)S(1)}, u32[]{:S(2)}, u32[]{:S(2)}) async-start(bf16[4,1024,128]{1,2,0:T(8,128)(2,1)} %pad_maximum_fusion), calls=%async_computation.1 | async-start | bytes 2097152 | tf_op jit(solution)/shard_map/all_to_all | solution.py:80
  44.0 43.8 %copy-start.10 = (f32[4,2]{1,0:T(4,128)S(1)}, f32[4,2]{1,0:T(4,128)}, u32[]{:S(2)}) copy-start(f32[4,2]{1,0:T(4,128)} %copy-done.9) | copy-start | bytes 100
  44.0 43.9 %copy-start.20 = (bf16[2048]{0:T(1024)(128)(2,1)S(1)}, bf16[2048]{0:T(1024)(128)(2,1)}, u32[]{:S(2)}) copy-start(bf16[2048]{0:T(1024)(128)(2,1)} %param.19) | copy-start | bytes 12292
  44.0 46.3 %copy-start.16 = (s32[256]{0:T(256)S(1)}, s32[256]{0:T(256)}, u32[]{:S(2)}) copy-start(s32[256]{0:T(256)} %param.17) | copy-start | bytes 3076
  44.0 154.2 %all-gather.8.cloned.1.call-start = ((), (), s32[]{:S(2)}) async-start(), calls=%async_computation.5 | async-start | bytes 5242880 | tf_op jit(solution)/shard_map/all_gather | solution.py:161
  44.1 53.0 %collective-permute-start.5 = (bf16[256,2048]{1,0:T(8,128)(2,1)S(1)}, bf16[256,2048]{1,0:T(8,128)(2,1)}, u32[]{:S(2)}, u32[]{:S(2)}) collective-permute-start(bf16[256,2048]{1,0:T(8,128)(2,1)S(1)} %copy-done.2), channel_id=1, source_target_pairs={{0,1},{1,0},{2,3},{3,2},{4,5},{5,4},{6,7},{7,6},{8,9},{9,8},{10,11... | collective-permute-start | bytes 3145736 | tf_op jit(solution)/shard_map/ppermute | solution.py:85
  46.7 44.2 %copy-start.4 = (bf16[256,256]{0,1:T(8,128)(2,1)S(1)}, bf16[256,256]{0,1:T(8,128)(2,1)}, u32[]{:S(2)}) copy-start(bf16[256,256]{0,1:T(8,128)(2,1)} %copy-done.3) | copy-start | bytes 393220
  58.4 7.2 %collective-permute-start.1 = (f32[4,72,64]{1,2,0:T(8,128)S(1)}, f32[4,72,64]{1,2,0:T(8,128)S(1)}, u32[]{:S(2)}, u32[]{:S(2)}) collective-permute-start(f32[4,72,64]{1,2,0:T(8,128)S(1)} %maximum_maximum_fusion.1), channel_id=1, source_target_pairs={{0,4},{2,6},{4,8},{6,10},{8,12},{10,14},{12,16},{14,18},{16,20},{1... | collective-permute-start | bytes 221192 | tf_op jit(solution)/shard_map/ppermute | solution.py:54
  67.0 1.0 copy-start
  68.0 167.3 %all-gather.4.cloned.1.call-start = ((), (), s32[]{:S(2)}) async-start(), calls=%async_computation.3 | async-start | bytes 4718592 | tf_op jit(solution)/shard_map/all_gather | solution.py:160
  69.5 14.3 %collective-permute-start.2 = (f32[4,72,64]{1,2,0:T(8,128)S(1)}, f32[4,72,64]{1,2,0:T(8,128)S(1)}, u32[]{:S(2)}, u32[]{:S(2)}) collective-permute-start(f32[4,72,64]{1,2,0:T(8,128)S(1)} %maximum_maximum_fusion.2), channel_id=1, source_target_pairs={{0,8},{2,10},{4,12},{6,14},{8,16},{10,18},{12,20},{14,22},{16,24},... | collective-permute-start | bytes 221192 | tf_op jit(solution)/shard_map/ppermute | solution.py:54
  77.5 19.6 %copy-start.5 = (bf16[128,2048]{1,0:T(8,128)(2,1)S(1)}, bf16[128,2048]{1,0:T(8,128)(2,1)}, u32[]{:S(2)}) copy-start(bf16[128,2048]{1,0:T(8,128)(2,1)} %param.11) | copy-start | bytes 1572868
  86.5 2.3 collective-permute-start.3
  92.8 4.3 %collective-permute-start.4 = (bf16[128,256]{1,0:T(8,128)(2,1)S(1)}, bf16[128,256]{1,0:T(8,128)(2,1)S(1)}, u32[]{:S(2)}, u32[]{:S(2)}) collective-permute-start(bf16[128,256]{1,0:T(8,128)(2,1)S(1)} %bitcast.101), channel_id=1, source_target_pairs={{0,1},{1,0},{2,3},{3,2},{4,5},{5,4},{6,7},{7,6},{8,9},{9,8},{10,11... | collective-permute-start | bytes 196616 | tf_op jit(solution)/shard_map/ppermute | solution.py:85
  99.7 201.2 %reduce-scatter.2.cloned.1.call-start = ((), (), s32[]{:S(2)}) async-start(), calls=%async_computation.6 | async-start | bytes 4718592 | tf_op jit(solution)/shard_map/reduce_scatter | solution.py:165
Sparse Core Ops, SparseCore 0:
  28.3 81.0 all-gather.5
  111.0 87.2 all-gather.7
  200.2 35.0 all-gather.3
  249.8 51.1 reduce-scatter.1
